TPU v7x, 32 devices: a whole 2x2x4 slice. The times are simulated.
32 devices in a mesh: grp: 2 (over y), ra: 4 (over z), cb: 4 (over x, core).
Axes of the slice: x: 2, y: 2, z: 4, core: 2. Of those that a mesh axis runs over, the one named last changes fastest.
Arguments:
- tokens: bfloat16 [1024, 4096], P('grp', 'ra'), parts along dimension 0, may hold values from -14 to 14
- pre_gain: bfloat16 [2, 4096], P(None, 'ra'), may hold values from 0.099609375 to 1.8984375
- post_gain: bfloat16 [2, 4096], P(None, 'ra'), may hold values from 0.099609375 to 1.8984375
- gate_weight: bfloat16 [2, 4096, 11008], P(None, 'ra', 'cb'), may hold values from -0.09375 to 0.09375
- up_weight: bfloat16 [2, 4096, 11008], P(None, 'ra', 'cb'), may hold values from -0.09375 to 0.09375
- gate_taps: bfloat16 [2, 3, 11008], P(None, None, 'cb'), may hold values from -3 to 3
- up_taps: bfloat16 [2, 3, 11008], P(None, None, 'cb'), may hold values from -3 to 3
- gate_bias: bfloat16 [2, 11008], P(None, 'cb'), may hold values from -3 to 3
- up_bias: bfloat16 [2, 11008], P(None, 'cb'), may hold values from -3 to 3
- down_weight: bfloat16 [2, 11008, 4096], P(None, 'cb', 'ra'), may hold values from -0.07624929 to 0.07624929
Outputs:
- layer_out: bfloat16 [1024, 4096], P('grp', 'ra'), parts along dimension 0
There are 2 independent parts, one for each index of `grp`. A program takes and returns all parts, laid end to end along the dimension named above; an argument that names none is the same for every part. Nothing has to cross between parts.
All inputs are finite; a program needn't handle non-finite values.
Results may differ from a plain program's by a relative error of at most 0.024.
Values may be sent and summed in bfloat16 or wider, within the bound.
A program may use at most 128 MiB of HBM per device.

v0:
```python
import jax
import jax.numpy as jnp
from jax import lax
from jax.sharding import PartitionSpec as P

D = 4096
LAYERS = 2
LEN = 256


epsilon = 1e-06
residual_scale = 0.5


def shifted_2(x, axis, by):
    size = lax.axis_size(axis)
    pairs = [(i, i + by) for i in range(size) if 0 <= i + by < size]
    return lax.ppermute(x, axis, pairs)


def rim_conv(values, rim_rows, tap_weights, positions):
    tap_count = tap_weights.shape[0]
    own_rows = values.shape[0]
    extended = jnp.concatenate([rim_rows, values], axis=0)
    result = tap_weights[tap_count - 1] * values
    for offset in range(1, tap_count):
        shifted = extended[tap_count - 1 - offset : tap_count - 1 - offset + own_rows]
        shifted = jnp.where((positions >= offset)[:, None], shifted, jnp.float32(0.0))
        result = result + tap_weights[tap_count - 1 - offset] * shifted
    return result


def local(
    tokens,
    pre_gain,
    post_gain,
    gate_weight,
    up_weight,
    gate_taps,
    up_taps,
    gate_bias,
    up_bias,
    down_weight,
):
    state = tokens
    for which_layer in range(LAYERS):
        widened = state.astype(jnp.float32)
        squares = jnp.sum(widened * widened, axis=1)
        normed = (widened * pre_gain[which_layer].astype(jnp.float32)).astype(jnp.bfloat16)
        gate_part = jnp.dot(normed, gate_weight[which_layer], preferred_element_type=jnp.float32)
        up_part = jnp.dot(normed, up_weight[which_layer], preferred_element_type=jnp.float32)
        gate_kernel = gate_taps[which_layer].astype(jnp.float32)
        up_kernel = up_taps[which_layer].astype(jnp.float32)
        gate_shift = gate_bias[which_layer].astype(jnp.float32)
        up_shift = up_bias[which_layer].astype(jnp.float32)
        down_rows = down_weight[which_layer]
        pre_total = lax.psum(squares, "ra")
        pre_scale = lax.rsqrt(pre_total / D + epsilon)[:, None]
        gate_sum, up_sum = (
            lax.psum_scatter(gate_part, "ra", scatter_dimension=0, tiled=True),
            lax.psum_scatter(up_part, "ra", scatter_dimension=0, tiled=True),
        )
        own_rows = gate_sum.shape[0]
        first_row = lax.axis_index("ra") * own_rows
        row_scale = lax.dynamic_slice_in_dim(pre_scale, first_row, own_rows, 0)
        gate_lin = gate_sum * row_scale
        up_lin = up_sum * row_scale
        rim_size = gate_kernel.shape[0] - 1
        gate_rim, up_rim = shifted_2(
            (gate_lin[own_rows - rim_size :], up_lin[own_rows - rim_size :]), "ra", 1
        )
        positions = (first_row + jnp.arange(own_rows, dtype=jnp.int32)) % LEN
        gate_conv = rim_conv(gate_lin, gate_rim, gate_kernel, positions) + gate_shift
        up_conv = rim_conv(up_lin, up_rim, up_kernel, positions) + up_shift
        hidden = (jax.nn.gelu(gate_conv, approximate=True) * up_conv).astype(jnp.bfloat16)
        partial_value = jnp.dot(
            lax.all_gather(hidden, "ra", axis=0, tiled=True),
            down_rows,
            preferred_element_type=jnp.float32,
        )
        branch = lax.psum(partial_value.astype(jnp.bfloat16), "cb").astype(jnp.float32)
        post_total = lax.psum(jnp.sum(branch * branch, axis=1), "ra")
        post_scale = lax.rsqrt(post_total / D + epsilon)[:, None]
        state = (
            residual_scale * widened
            + branch * post_scale * post_gain[which_layer].astype(jnp.float32)
        ).astype(jnp.bfloat16)
    return state


def solution(mesh):
    in_specs = (
        P("grp", "ra"),
        P(None, "ra"),
        P(None, "ra"),
        P(None, "ra", "cb"),
        P(None, "ra", "cb"),
        P(None, None, "cb"),
        P(None, None, "cb"),
        P(None, "cb"),
        P(None, "cb"),
        P(None, "cb", "ra"),
    )
    out_specs = P("grp", "ra")
    return jax.shard_map(local, mesh=mesh, in_specs=in_specs, out_specs=out_specs, check_vma=False)
```

profile of v0, /device:TPU:0, one launch (start us, length us, event | category | flops | bytes accessed | tf_op | source)
XLA Modules:
  0.0 724.2 jit_solution(2792509699364720131)
XLA Ops:
  7.3 8.5 %fusion.10 = f32[512,2752]{0,1:T(8,128)} fusion(bf16[2,1024,2752]{1,2,0:T(8,128)(2,1)} %param.13, bf16[512,1024]{1,0:T(8,128)(2,1)} %param.10, f32[1024]{0:T(1024)S(1)} %bitcast.32), kind=kOutput, calls=%fused_computation.10 | convolution fusion | flops 2887254016 | bytes 12324864 | tf_op jit(solution)/shard_map/dot_general | solution.py:50
  17.0 7.7 %fusion.8 = f32[512,2752]{0,1:T(8,128)} fusion(bf16[2,1024,2752]{1,2,0:T(8,128)(2,1)} %param.14, bf16[512,1024]{1,0:T(8,128)(2,1)S(1)} %copy-done, f32[1024]{0:T(1024)S(1)} %bitcast.33), kind=kOutput, calls=%fused_computation.8 | convolution fusion | flops 2887254016 | bytes 12324864 | tf_op jit(solution)/shard_map/dot_general | solution.py:51
  25.1 14.0 %psum.42 = f32[512]{0:T(512)S(1)} all-reduce(f32[512]{0:T(512)S(1)} %fusion.27), channel_id=1, replica_groups=mesh['grp'=2,'ra'=4,'cb'=4] {'ra'}, use_global_device_ids=true, to_apply=%region_2.0 | all-reduce | flops 512 | bytes 4096 | tf_op jit(solution)/shard_map/psum | solution.py:57
  39.6 79.5 %reduce-scatter.5.cloned.1.call-done = f32[128,2752]{0,1:T(8,128)} async-done(((f32[512,2752]{0,1:T(8,128)}), f32[128,2752]{0,1:T(8,128)}) %reduce-scatter.5.cloned.1.call-update) | async-done | bytes 1409040 | tf_op jit(solution)/shard_map/reduce_scatter | solution.py:60
  119.1 103.0 %reduce-scatter.7.cloned.1.call-done = f32[128,2752]{0,1:T(8,128)} async-done(((f32[512,2752]{0,1:T(8,128)}), f32[128,2752]{0,1:T(8,128)}) %reduce-scatter.7.cloned.1.call-update) | async-done | bytes 1409040 | tf_op jit(solution)/shard_map/reduce_scatter | solution.py:61
  222.1 2.0 broadcast_multiply_fusion.3
  225.6 1.8 copy.13
  227.4 3.4 collective-permute-start.1
  232.3 1.8 copy.11
  234.1 3.9 collective-permute-start
  241.2 9.2 %fusion.44 = bf16[128,2752]{0,1:T(8,128)(2,1)} fusion(f32[2,2752]{0,1:T(8,128)} %copy.14, f32[128,2752]{0,1:T(8,128)S(1)} %get-tuple-element.34, f32[2,2752]{0,1:T(8,128)} %copy.12, f32[128,2752]{0,1:T(8,128)S(1)} %get-tuple-element.33, f32[2752]{0:T(1024)S(1)} %get-tuple-element.20, f32[2752]{0:T(1024)S(1)} %get-tuple-element.15, ...), kind=kLoop, calls=%fused_computation.60 | loop fusion | flops 10567680 | bytes 3654912 | tf_op jit(solution)/shard_map/convert_element_type | solution.py:75
  250.5 57.9 %all-gather.3.cloned.1.call-done = bf16[512,2752]{0,1:T(8,128)(2,1)} async-done(((bf16[128,2752]{0,1:T(8,128)(2,1)}), bf16[512,2752]{0,1:T(8,128)(2,1)}) %all-gather.3.cloned.1.call-update) | async-done | bytes 2818064 | tf_op jit(solution)/shard_map/all_gather | solution.py:77
  308.4 7.6 %fusion.30 = bf16[512,1024]{1,0:T(8,128)(2,1)} fusion(bf16[512,2752]{0,1:T(8,128)(2,1)} %all-gather.3.cloned.1.call-done, bf16[2,2752,1024]{2,1,0:T(8,128)(2,1)} %param.19), kind=kOutput, calls=%fused_computation.50 | convolution fusion | flops 2886205440 | bytes 9502720 | tf_op jit(solution)/shard_map/dot_general | solution.py:76
  316.1 34.6 %all-reduce.3.cloned.1.call-done = bf16[512,1024]{1,0:T(8,128)(2,1)} async-done(((bf16[512,1024]{1,0:T(8,128)(2,1)}), bf16[512,1024]{1,0:T(8,128)(2,1)}) %all-reduce.3.cloned.1.call-update) | async-done | bytes 1048592 | tf_op jit(solution)/shard_map/psum | solution.py:81
  350.7 1.6 fusion.18
  352.3 11.9 %psum.44 = f32[512]{0:T(512)S(1)} all-reduce(f32[512]{0:T(512)S(1)} %fusion.18), channel_id=1, replica_groups=mesh['grp'=2,'ra'=4,'cb'=4] {'ra'}, use_global_device_ids=true, to_apply=%region_6.7 | all-reduce | flops 512 | bytes 4096 | tf_op jit(solution)/shard_map/psum | solution.py:82
  364.9 8.0 %fusion.4 = f32[512,2752]{0,1:T(8,128)} fusion(bf16[2,1024,2752]{1,2,0:T(8,128)(2,1)} %param.13, bf16[512,1024]{1,0:T(8,128)(2,1)S(1)} %get-tuple-element.22, f32[1024]{0:T(1024)S(1)} %bitcast.30), kind=kOutput, calls=%fused_computation.4 | convolution fusion | flops 2887254016 | bytes 12324864 | tf_op jit(solution)/shard_map/dot_general | solution.py:50
  373.0 7.7 %fusion.2 = f32[512,2752]{0,1:T(8,128)} fusion(bf16[2,1024,2752]{1,2,0:T(8,128)(2,1)} %param.14, bf16[512,1024]{1,0:T(8,128)(2,1)S(1)} %get-tuple-element.22, f32[1024]{0:T(1024)S(1)} %bitcast.31), kind=kOutput, calls=%fused_computation.2 | convolution fusion | flops 2887254016 | bytes 12324864 | tf_op jit(solution)/shard_map/dot_general | solution.py:51
  380.7 10.1 %psum.45 = f32[512]{0:T(512)S(1)} all-reduce(f32[512]{0:T(512)S(1)} %get-tuple-element.21), channel_id=1, replica_groups=mesh['grp'=2,'ra'=4,'cb'=4] {'ra'}, use_global_device_ids=true, to_apply=%region_9.10 | all-reduce | flops 512 | bytes 4096 | tf_op jit(solution)/shard_map/psum | solution.py:57
  390.9 80.3 %reduce-scatter.9.cloned.1.call-done = f32[128,2752]{0,1:T(8,128)} async-done(((f32[512,2752]{0,1:T(8,128)}), f32[128,2752]{0,1:T(8,128)}) %reduce-scatter.9.cloned.1.call-update) | async-done | bytes 1409040 | tf_op jit(solution)/shard_map/reduce_scatter | solution.py:60
  471.2 102.9 %reduce-scatter.11.cloned.1.call-done = f32[128,2752]{0,1:T(8,128)} async-done(((f32[512,2752]{0,1:T(8,128)}), f32[128,2752]{0,1:T(8,128)}) %reduce-scatter.11.cloned.1.call-update) | async-done | bytes 1409040 | tf_op jit(solution)/shard_map/reduce_scatter | solution.py:61
  574.1 2.0 broadcast_multiply_fusion.1
  577.6 1.8 copy.17
  579.4 3.4 collective-permute-start.3
  584.3 1.8 copy.15
  586.1 3.9 collective-permute-start.2
  593.3 9.2 %fusion.53 = bf16[128,2752]{0,1:T(8,128)(2,1)} fusion(f32[2,2752]{0,1:T(8,128)} %copy.18, f32[128,2752]{0,1:T(8,128)S(1)} %get-tuple-element.32, f32[2,2752]{0,1:T(8,128)} %copy.16, f32[128,2752]{0,1:T(8,128)S(1)} %get-tuple-element.31, f32[2752]{0:T(1024)S(1)} %get-tuple-element.19, f32[2752]{0:T(1024)S(1)} %get-tuple-element.9, ...), kind=kLoop, calls=%fused_computation.69 | loop fusion | flops 10567680 | bytes 3654912 | tf_op jit(solution)/shard_map/convert_element_type | solution.py:75
  602.6 57.8 %all-gather.5.cloned.1.call-done = bf16[512,2752]{0,1:T(8,128)(2,1)} async-done(((bf16[128,2752]{0,1:T(8,128)(2,1)}), bf16[512,2752]{0,1:T(8,128)(2,1)}) %all-gather.5.cloned.1.call-update) | async-done | bytes 2818064 | tf_op jit(solution)/shard_map/all_gather | solution.py:77
  660.3 7.6 %fusion.33 = bf16[512,1024]{1,0:T(8,128)(2,1)} fusion(bf16[512,2752]{0,1:T(8,128)(2,1)} %all-gather.5.cloned.1.call-done, bf16[2,2752,1024]{2,1,0:T(8,128)(2,1)} %param.19), kind=kOutput, calls=%fused_computation.51 | convolution fusion | flops 2886205440 | bytes 9502720 | tf_op jit(solution)/shard_map/dot_general | solution.py:76
  668.0 34.6 %all-reduce.5.cloned.1.call-done = bf16[512,1024]{1,0:T(8,128)(2,1)} async-done(((bf16[512,1024]{1,0:T(8,128)(2,1)}), bf16[512,1024]{1,0:T(8,128)(2,1)}) %all-reduce.5.cloned.1.call-update) | async-done | bytes 1048592 | tf_op jit(solution)/shard_map/psum | solution.py:81
  702.6 1.6 fusion.22
  704.2 11.7 %psum.47 = f32[512]{0:T(512)S(1)} all-reduce(f32[512]{0:T(512)S(1)} %fusion.22), channel_id=1, replica_groups=mesh['grp'=2,'ra'=4,'cb'=4] {'ra'}, use_global_device_ids=true, to_apply=%region_13.14 | all-reduce | flops 512 | bytes 4096 | tf_op jit(solution)/shard_map/psum | solution.py:82
  (67 shorter events, 18.0 us)
Async XLA Ops:
  6.5 112.6 %reduce-scatter.5.cloned.1.call-start = ((), (), s32[]{:S(2)}) async-start(), calls=%async_computation.4 | async-start | bytes 7045120 | tf_op jit(solution)/shard_map/reduce_scatter | solution.py:60
  15.8 1.2 copy-start
  15.8 206.3 %reduce-scatter.7.cloned.1.call-start = ((), (), s32[]{:S(2)}) async-start(), calls=%async_computation.5 | async-start | bytes 7045120 | tf_op jit(solution)/shard_map/reduce_scatter | solution.py:61
  24.7 14.5 %copy-start.8 = (bf16[2,2752]{1,0:T(2,128)(2,1)S(1)}, bf16[2,2752]{1,0:T(2,128)(2,1)}, u32[]{:S(2)}) copy-start(bf16[2,2752]{1,0:T(2,128)(2,1)} %param.18) | copy-start | bytes 33028
  24.7 14.5 %copy-start.9 = (bf16[2,2752]{1,0:T(2,128)(2,1)S(1)}, bf16[2,2752]{1,0:T(2,128)(2,1)}, u32[]{:S(2)}) copy-start(bf16[2,2752]{1,0:T(2,128)(2,1)} %param.17) | copy-start | bytes 33028
  24.7 14.6 %copy-start.6 = (bf16[2,3,2752]{2,0,1:T(2,128)(2,1)S(1)}, bf16[2,3,2752]{2,0,1:T(2,128)(2,1)}, u32[]{:S(2)}) copy-start(bf16[2,3,2752]{2,0,1:T(2,128)(2,1)} %param.16) | copy-start | bytes 99076
  24.7 14.7 %copy-start.7 = (bf16[2,3,2752]{2,0,1:T(2,128)(2,1)S(1)}, bf16[2,3,2752]{2,0,1:T(2,128)(2,1)}, u32[]{:S(2)}) copy-start(bf16[2,3,2752]{2,0,1:T(2,128)(2,1)} %param.15) | copy-start | bytes 99076
  24.7 283.7 %all-gather.3.cloned.1.call-start = ((), (), s32[]{:S(2)}) async-start(), calls=%async_computation.6 | async-start | bytes 3522560 | tf_op jit(solution)/shard_map/all_gather | solution.py:77
  227.4 10.7 %collective-permute-start.1 = (f32[2,2752]{1,0:T(2,128)S(1)}, f32[2,2752]{1,0:T(2,128)S(1)}, u32[]{:S(2)}, u32[]{:S(2)}) collective-permute-start(f32[2,2752]{1,0:T(2,128)S(1)} %copy.13), channel_id=1, source_target_pairs={{0,4},{4,8},{8,12},{1,5},{5,9},{9,13},{2,6},{6,10},{10,14},{3,7},{... | collective-permute-start | bytes 66056 | tf_op jit(solution)/shard_map/ppermute | solution.py:18
  234.1 5.5 collective-permute-start
  250.4 65.6 %copy-start.10 = (bf16[2,1024]{1,0:T(2,128)(2,1)S(1)}, bf16[2,1024]{1,0:T(2,128)(2,1)}, u32[]{:S(2)}) copy-start(bf16[2,1024]{1,0:T(2,128)(2,1)} %param.12) | copy-start | bytes 12292
  250.5 100.2 %all-reduce.3.cloned.1.call-start = ((), (), s32[]{:S(2)}) async-start(), calls=%async_computation.7 | async-start | bytes 2097152 | tf_op jit(solution)/shard_map/psum | solution.py:81
  316.0 48.1 %copy-start.1 = (bf16[512,1024]{1,0:T(8,128)(2,1)S(1)}, bf16[512,1024]{1,0:T(8,128)(2,1)}, u32[]{:S(2)}) copy-start(bf16[512,1024]{1,0:T(8,128)(2,1)} %param.10) | copy-start | bytes 3145732
  316.0 155.2 %reduce-scatter.9.cloned.1.call-start = ((), (), s32[]{:S(2)}) async-start(), calls=%async_computation.8 | async-start | bytes 7045120 | tf_op jit(solution)/shard_map/reduce_scatter | solution.py:60
  350.7 13.5 %copy-start.4 = (bf16[512,1024]{1,0:T(8,128)(2,1)S(1)}, bf16[512,1024]{1,0:T(8,128)(2,1)}, u32[]{:S(2)}) copy-start(bf16[512,1024]{1,0:T(8,128)(2,1)} %all-reduce.3.cloned.1.call-done) | copy-start | bytes 3145732
  364.9 8.1 %copy-start.2 = (bf16[512,1024]{1,0:T(8,128)(2,1)}, bf16[512,1024]{1,0:T(8,128)(2,1)S(1)}, u32[]{:S(2)}) copy-start(bf16[512,1024]{1,0:T(8,128)(2,1)S(1)} %get-tuple-element.22) | copy-start | bytes 3145732
  372.9 201.2 %reduce-scatter.11.cloned.1.call-start = ((), (), s32[]{:S(2)}) async-start(), calls=%async_computation.9 | async-start | bytes 7045120 | tf_op jit(solution)/shard_map/reduce_scatter | solution.py:61
  380.7 279.7 %all-gather.5.cloned.1.call-start = ((), (), s32[]{:S(2)}) async-start(), calls=%async_computation.10 | async-start | bytes 3522560 | tf_op jit(solution)/shard_map/all_gather | solution.py:77
  579.4 10.8 %collective-permute-start.3 = (f32[2,2752]{1,0:T(2,128)S(1)}, f32[2,2752]{1,0:T(2,128)S(1)}, u32[]{:S(2)}, u32[]{:S(2)}) collective-permute-start(f32[2,2752]{1,0:T(2,128)S(1)} %copy.17), channel_id=1, source_target_pairs={{0,4},{4,8},{8,12},{1,5},{5,9},{9,13},{2,6},{6,10},{10,14},{3,7},{... | collective-permute-start | bytes 66056 | tf_op jit(solution)/shard_map/ppermute | solution.py:18
  586.1 5.7 collective-permute-start.2
  602.5 100.1 %all-reduce.5.cloned.1.call-start = ((), (), s32[]{:S(2)}) async-start(), calls=%async_computation.11 | async-start | bytes 2097152 | tf_op jit(solution)/shard_map/psum | solution.py:81
  667.9 48.0 %copy-start.3 = (bf16[512,1024]{1,0:T(8,128)(2,1)S(1)}, bf16[512,1024]{1,0:T(8,128)(2,1)}, u32[]{:S(2)}) copy-start(bf16[512,1024]{1,0:T(8,128)(2,1)} %copy-done.2) | copy-start | bytes 3145732
  702.6 13.3 %copy-start.5 = (bf16[512,1024]{1,0:T(8,128)(2,1)S(1)}, bf16[512,1024]{1,0:T(8,128)(2,1)}, u32[]{:S(2)}) copy-start(bf16[512,1024]{1,0:T(8,128)(2,1)} %all-reduce.5.cloned.1.call-done) | copy-start | bytes 3145732
Sparse Core Ops, SparseCore 0:
  16.0 103.1 reduce-scatter.4
  121.5 100.6 reduce-scatter.6
  250.6 57.8 all-gather.2
  316.1 34.4 all-reduce.2
  373.0 98.1 reduce-scatter.8
  473.4 100.6 reduce-scatter.10
  602.7 57.6 all-gather.4
  668.1 34.4 all-reduce.4
where the time goes:
time: 725 us; the launch traced here: 724 us
  waiting for transfers between devices  551 us (76%)
  blocking collectives  47.6 us (7%)
  matrix products  47 us (6%)
  other arithmetic  29 us (4%)
  local copies, waits for them, and re-layouts  21.2 us (3%)
  starting transfers between devices  14.9 us (2%)
  between operations  13.7 us (2%)
    reduce_scatter x2, waiting for transfers between devices, local(): lax.psum_scatter(up_part, 'ra', scatter_dimension=0, tiled=True)  206 us
    reduce_scatter x2, waiting for transfers between devices, local(): lax.psum_scatter(gate_part, 'ra', scatter_dimension=0, tiled=True)  160 us
    all_gather x2, waiting for transfers between devices, local(): lax.all_gather(hidden, 'ra', axis=0, tiled=True)  116 us
    psum x2, waiting for transfers between devices, local(): lax.psum(partial_value.astype(jnp.bfloat16), 'cb').astype(jnp.float32)  69.2 us
    psum x2, blocking collectives, local(): pre_total = lax.psum(squares, 'ra')  24.1 us
    psum x2, blocking collectives, local(): post_total = lax.psum(jnp.sum(branch * branch, axis=1), 'ra')  23.6 us
    convert_element_type x2, other arithmetic, local(): (jax.nn.gelu(gate_conv, approximate=True) * up_conv).astype(jnp.bfloat16)  18.4 us
    dot_general x2, matrix products, local(): jnp.dot(normed, gate_weight[which_layer], preferred_element_type=jnp.floa...  16.5 us
  transfers between devices with their start and end apart: 12, of which 8 were waited for; matrix products, arithmetic and copies ran while one was open for 4% of the time, Pallas kernels for 0%

commit v1 on v0

v1 whole, which is shorter than its diff:
```python
import functools

import jax
import jax.numpy as jnp
from jax import lax
from jax.experimental import pallas as pl
from jax.experimental.pallas import tpu as pltpu
from jax.sharding import PartitionSpec as P

LEN = 256
LANES = 128
SKEW = 2

epsilon = 1e-06
residual_scale = 0.5
MESH = pl.DeviceIdType.MESH


def hidden_kernel(
    layer, n, nch, nfull, fl,
    x_ref, scale_ref, coef_ref, tg_ref, tu_ref, wg_hbm, wu_hbm, wd_hbm,
    out_ref,
    w, wd, part, hid, acc, wsem, wdsem, part_send, part_recv, hid_send, hid_recv,
):
    z = lax.axis_index("ra")
    half = x_ref.shape[0] // 2

    def w_copies(j):
        cols = pl.ds(pl.multiple_of(j * LANES, LANES), LANES)
        return (
            pltpu.make_async_copy(
                wg_hbm.at[layer, :, cols], w.at[j, :, pl.ds(0, LANES)], wsem.at[0, j]),
            pltpu.make_async_copy(
                wu_hbm.at[layer, :, cols], w.at[j, :, pl.ds(LANES, LANES)], wsem.at[1, j]),
        )

    @pl.loop(0, nfull)
    def _(j):
        for copy in w_copies(j):
            copy.start()

    wd_copy = pltpu.make_async_copy(wd_hbm.at[layer], wd.at[pl.ds(0, fl)], wdsem)
    wd_copy.start()

    barrier = pltpu.get_barrier_semaphore()

    @pl.when(z > 0)
    def _():
        pl.semaphore_signal(barrier, inc=1, device_id={"ra": z - 1}, device_id_type=MESH)

    @pl.when(z < n - 1)
    def _():
        pl.semaphore_signal(barrier, inc=1, device_id={"ra": z + 1}, device_id_type=MESH)

    if nch > nfull:
        w[nfull, :, 0:LANES] = tg_ref[...]
        w[nfull, :, LANES:] = tu_ref[...]
        wd[fl:, :] = jnp.zeros((nch * LANES - fl, wd.shape[1]), wd.dtype)
    acc[...] = jnp.zeros_like(acc)

    inner = (z > 0) & (z < n - 1)

    @pl.when(inner)
    def _():
        pl.semaphore_wait(barrier, 2)

    @pl.when(jnp.logical_not(inner))
    def _():
        pl.semaphore_wait(barrier, 1)

    def place(d):
        if d == 0:
            return n - 1 - z, z - 1, z + 1
        return z, z + 1, z - 1

    def part_copy(d, j, target):
        return pltpu.make_async_remote_copy(
            src_ref=part.at[d, j], dst_ref=part.at[d, j],
            send_sem=part_send.at[d, j], recv_sem=part_recv.at[d, j],
            device_id={"ra": target}, device_id_type=MESH)

    def hid_copy(d, j, target):
        return pltpu.make_async_remote_copy(
            src_ref=hid.at[d, j], dst_ref=hid.at[d, j],
            send_sem=hid_send.at[d, j], recv_sem=hid_recv.at[d, j],
            device_id={"ra": target}, device_id_type=MESH)

    def conv(values, taps, bias):
        rows = lax.broadcasted_iota(jnp.int32, values.shape, 0) % LEN
        count = len(taps)
        result = taps[count - 1] * values
        for offset in range(1, count):
            moved = jnp.where(rows >= offset, pltpu.roll(values, offset, 0), 0.0)
            result = result + taps[count - 1 - offset] * moved
        return result + bias

    def add_down(d, j):
        rows = slice(d * half, (d + 1) * half)
        wrows = pl.ds(pl.multiple_of(j * LANES, LANES), LANES)
        acc[rows, :] += jnp.dot(hid[d, j], wd[wrows, :], preferred_element_type=jnp.float32)

    @pl.loop(0, nch + 2 * (n - 1) * SKEW)
    def _(s):
        @pl.when(s < nfull)
        def _():
            for copy in w_copies(s):
                copy.wait()

        @pl.when(s == 1)
        def _():
            wd_copy.wait()

        for d in range(2):
            p, nxt, prv = place(d)
            rows = slice(d * half, (d + 1) * half)
            c = s - p * SKEW

            @pl.when((c >= 0) & (c < nch))
            def _():
                own = jnp.dot(x_ref[rows, :], w[c], preferred_element_type=jnp.float32)

                @pl.when(p == 0)
                def _():
                    part[d, c] = own.astype(part.dtype)
                    part_copy(d, c, nxt).start()

                @pl.when((p > 0) & (p < n - 1))
                def _():
                    part_copy(d, c, nxt).wait_recv()
                    part[d, c] = (part[d, c].astype(jnp.float32) + own).astype(part.dtype)
                    part_copy(d, c, nxt).start()

                @pl.when(p == n - 1)
                def _():
                    part_copy(d, c, prv).wait_recv()
                    total = (part[d, c].astype(jnp.float32) + own) * scale_ref[rows, :]
                    coef = coef_ref[:, pl.ds(pl.multiple_of(c * LANES, LANES), LANES)]
                    k = coef.shape[0] // 2
                    row = [coef[i : i + 1, :] for i in range(2 * k)]
                    gate = conv(total[:, :LANES], row[: k - 1], row[k - 1])
                    up = conv(total[:, LANES:], row[k : 2 * k - 1], row[2 * k - 1])
                    hid[d, c] = (jax.nn.gelu(gate, approximate=True) * up).astype(hid.dtype)
                    hid_copy(d, c, prv).start()
                    add_down(d, c)

            e = s - (2 * (n - 1) - p) * SKEW

            @pl.when((p < n - 1) & (e >= 0) & (e < nch))
            def _():
                hid_copy(d, e, nxt).wait_recv()

                @pl.when(p > 0)
                def _():
                    hid_copy(d, e, prv).start()

                add_down(d, e)

    out_ref[...] = acc[...].astype(out_ref.dtype)

    for d in range(2):
        p, nxt, prv = place(d)

        @pl.loop(0, nch)
        def _(j):
            @pl.when(p < n - 1)
            def _():
                part_copy(d, j, nxt).wait_send()

            @pl.when(p > 0)
            def _():
                hid_copy(d, j, prv).wait_send()


def down_partial(layer, n, normed, scale, coef, tg, tu, gate_weight, up_weight, down_weight):
    tokens, dl = normed.shape
    fl = gate_weight.shape[2]
    nfull = fl // LANES
    nch = -(-fl // LANES)
    half = tokens // 2
    vmem = pl.BlockSpec(memory_space=pltpu.VMEM)
    hbm = pl.BlockSpec(memory_space=pl.ANY)
    dma = pltpu.SemaphoreType.DMA
    return pl.pallas_call(
        functools.partial(hidden_kernel, layer, n, nch, nfull, fl),
        out_shape=jax.ShapeDtypeStruct((tokens, down_weight.shape[2]), jnp.bfloat16),
        in_specs=[vmem] * 5 + [hbm] * 3,
        out_specs=vmem,
        scratch_shapes=[
            pltpu.VMEM((nch, dl, 2 * LANES), jnp.bfloat16),
            pltpu.VMEM((nch * LANES, down_weight.shape[2]), jnp.bfloat16),
            pltpu.VMEM((2, nch, half, 2 * LANES), jnp.bfloat16),
            pltpu.VMEM((2, nch, half, LANES), jnp.bfloat16),
            pltpu.VMEM((tokens, down_weight.shape[2]), jnp.float32),
            dma((2, nch)),
            dma,
            dma((2, nch)),
            dma((2, nch)),
            dma((2, nch)),
            dma((2, nch)),
        ],
        compiler_params=pltpu.CompilerParams(
            collective_id=layer, has_side_effects=True, vmem_limit_bytes=56 * 1024 * 1024
        ),
        name=f"hidden_{layer}",
    )(normed, scale, coef, tg, tu, gate_weight, up_weight, down_weight)


def local(
    n,
    tokens,
    pre_gain,
    post_gain,
    gate_weight,
    up_weight,
    gate_taps,
    up_taps,
    gate_bias,
    up_bias,
    down_weight,
):
    width = tokens.shape[1] * n
    fl = gate_weight.shape[2]
    padding = -fl % LANES
    cut = fl // LANES * LANES
    pad_cols = lambda a: jnp.pad(a, ((0, 0),) * (a.ndim - 1) + ((0, padding),))
    if padding:
        tail = lambda a: jnp.pad(a[:, :, cut:], ((0, 0), (0, 0), (0, LANES - (fl - cut))))
        tails_gate, tails_up = tail(gate_weight), tail(up_weight)
    else:
        tails_gate = tails_up = jnp.zeros((gate_weight.shape[0], 16, LANES), jnp.bfloat16)
    coefs = pad_cols(
        jnp.concatenate(
            [gate_taps, gate_bias[:, None], up_taps, up_bias[:, None]], axis=1
        ).astype(jnp.float32)
    )
    state = tokens
    for layer in range(gate_weight.shape[0]):
        widened = state.astype(jnp.float32)
        pre_total = lax.psum(jnp.sum(widened * widened, axis=1), "ra")
        pre_scale = lax.rsqrt(pre_total / width + epsilon)[:, None]
        normed = (widened * pre_gain[layer].astype(jnp.float32)).astype(jnp.bfloat16)
        partial_value = down_partial(
            layer, n, normed, pre_scale, coefs[layer], tails_gate[layer], tails_up[layer],
            gate_weight, up_weight, down_weight,
        )
        branch = lax.psum(partial_value, "cb").astype(jnp.float32)
        post_total = lax.psum(jnp.sum(branch * branch, axis=1), "ra")
        post_scale = lax.rsqrt(post_total / width + epsilon)[:, None]
        state = (
            residual_scale * widened
            + branch * post_scale * post_gain[layer].astype(jnp.float32)
        ).astype(jnp.bfloat16)
    return state


def solution(mesh):
    in_specs = (
        P("grp", "ra"),
        P(None, "ra"),
        P(None, "ra"),
        P(None, "ra", "cb"),
        P(None, "ra", "cb"),
        P(None, None, "cb"),
        P(None, None, "cb"),
        P(None, "cb"),
        P(None, "cb"),
        P(None, "cb", "ra"),
    )
    body = functools.partial(local, mesh.shape["ra"])
    return jax.shard_map(
        body, mesh=mesh, in_specs=in_specs, out_specs=P("grp", "ra"), check_vma=False
    )
```

time: 725 us -> 417 us (0.58)
  waiting for transfers between devices: 551 us -> 69.8 us
  Pallas kernels: 0 us -> 237 us
  matrix products: 47 us -> 0 us
  local copies, waits for them, and re-layouts: 21.2 us -> 38.4 us
  other arithmetic: 29 us -> 12.3 us
  starting transfers between devices: 14.9 us -> 0.04 us
    reduce_scatter x4 -> x0, waiting for transfers between devices: 366 us -> none  [the longest x2 206 us: local(): lax.psum_scatter(up_part, 'ra', scatter_dimension=0, tiled=True)]
    pallas_call x0 -> x2, Pallas kernels: none -> 237 us  [down_partial(): pl.pallas_call(functools.partial(hidden_kernel, layer, n, nch, nfull, fl)...]
    all_gather x2 -> x0, waiting for transfers between devices: 116 us -> none  [local(): lax.all_gather(hidden, 'ra', axis=0, tiled=True)]
    dot_general x6 -> x0, matrix products: 47 us -> none  [the longest x2 16.5 us: local(): jnp.dot(normed, gate_weight[which_layer], preferred_element_type=jnp.floa...]
    unnamed x22 -> x8, local copies, waits for them, and re-layouts: 1.19 us -> 32.3 us
    convert_element_type x5 -> x2, other arithmetic: 19.9 us -> 3.88 us  [the longest x1 2.67 us: local(): state = (residual_scale * widened + branch * post_scale * post_gain[layer...]
    ppermute x4 -> x0, starting transfers between devices: 14.6 us -> none  [shifted_2(): return lax.ppermute(x, axis, pairs)]
    slice x10 -> x3, local copies, waits for them, and re-layouts: 13.6 us -> 1.08 us  [local(): a[:, :, cut:]]
  transfers between devices with their start and end apart: 12 -> 2, of which waited for: 8 -> 2; matrix products, arithmetic and copies ran while one was open for 4% -> 0% of each run, Pallas kernels for 0% -> 0%
where the time goes in v1:
time: 417 us; the launch traced here: 416 us
  Pallas kernels  237 us (57%)
  waiting for transfers between devices  69.8 us (17%)
  blocking collectives  45.2 us (11%)
  local copies, waits for them, and re-layouts  38.4 us (9%)
  between operations  13.5 us (3%)
  other arithmetic  12.3 us (3%)
    pallas_call x2, Pallas kernels, down_partial(): pl.pallas_call(functools.partial(hidden_kernel, layer, n, nch, nfull, fl)...  237 us
    psum x2, waiting for transfers between devices, local(): branch = lax.psum(partial_value, 'cb').astype(jnp.float32)  69.7 us
    unnamed x8, local copies, waits for them, and re-layouts  32.3 us
    psum x2, blocking collectives, local(): post_total = lax.psum(jnp.sum(branch * branch, axis=1), 'ra')  23.4 us
    psum x2, blocking collectives, local(): pre_total = lax.psum(jnp.sum(widened * widened, axis=1), 'ra')  21.8 us
  transfers between devices with their start and end apart: 2, of which 2 were waited for; matrix products, arithmetic and copies ran while one was open for 0% of the time, Pallas kernels for 0%

profile of v1, /device:TPU:0, one launch (start us, length us, event | category | flops | bytes accessed | tf_op | source)
XLA Modules:
  0.0 415.9 jit_solution(14200394669566002524)
XLA Ops:
  6.5 0.8 slice_convert_fusion.1
  7.3 0.7 copy.20
  8.0 0.7 copy.22
  8.8 0.8 copy.19
  9.5 0.8 copy.21
  10.3 0.1 fusion.23
  10.4 0.7 slice_bitcast_fusion
  11.1 2.5 fusion.9
  13.6 13.5 %psum.42 = f32[512]{0:T(512)S(1)} all-reduce(f32[512]{0:T(512)S(1)} %get-tuple-element.7), channel_id=1, replica_groups=mesh['grp'=2,'ra'=4,'cb'=4] {'ra'}, use_global_device_ids=true, to_apply=%region_1.2 | all-reduce | flops 512 | bytes 4096 | tf_op jit(solution)/shard_map/psum | solution.py:239
  27.1 0.9 copy.25.scale_ref
  28.0 15.5 %copy.23.wg_hbm = bf16[2,1024,2752]{2,1,0:T(8,128)(2,1)} copy(bf16[2,1024,2752]{1,2,0:T(8,128)(2,1)} %param.13) | data formatting | bytes 22544384 | tf_op args[3]
  43.4 15.3 %copy.24.wu_hbm = bf16[2,1024,2752]{2,1,0:T(8,128)(2,1)} copy(bf16[2,1024,2752]{1,2,0:T(8,128)(2,1)} %param.14) | data formatting | bytes 22544384 | tf_op args[4]
  58.7 1.1 slice.50
  59.8 1.2 fusion.13
  61.0 117.4 %hidden_0.1 = bf16[512,1024]{1,0:T(8,128)(2,1)} custom-call(bf16[512,1024]{1,0:T(8,128)(2,1)} %get-tuple-element.8.x_ref, f32[512,1]{1,0:T(8,128)} %copy.25.scale_ref, f32[8,2816]{1,0:T(8,128)} %get-tuple-element.14.coef_ref, bf16[1024,128]{1,0:T(8,128)(2,1)} %get-tuple-element.12.tg_ref, bf16[1024,128]{1,0:T(8,128)(2,1)} %get-tuple-element.19.tu_ref, ...), custom_call_target="tpu_custom_call" | custom-call | tf_op jit(solution)/shard_map/hidden_0/pallas_call | solution.py:183
  178.3 0.0 copy-start
  178.3 0.0 all-reduce.6.cloned.1.call-update
  178.4 0.0 all-reduce.8.cloned.1.call-start
  178.4 35.3 %all-reduce.6.cloned.1.call-done = bf16[512,1024]{1,0:T(8,128)(2,1)} async-done(((bf16[512,1024]{1,0:T(8,128)(2,1)}), bf16[512,1024]{1,0:T(8,128)(2,1)}) %all-reduce.6.cloned.1.call-update) | async-done | bytes 1048592 | tf_op jit(solution)/shard_map/psum | solution.py:246
  213.8 1.5 fusion
  215.3 11.7 %psum.44 = f32[512]{0:T(512)S(1)} all-reduce(f32[512]{0:T(512)S(1)} %fusion), channel_id=1, replica_groups=mesh['grp'=2,'ra'=4,'cb'=4] {'ra'}, use_global_device_ids=true, to_apply=%region_4.5 | all-reduce | flops 512 | bytes 4096 | tf_op jit(solution)/shard_map/psum | solution.py:247
  227.0 0.0 copy-done
  227.0 2.0 fusion.11
  228.9 8.4 %psum.45 = f32[512]{0:T(512)S(1)} all-reduce(f32[512]{0:T(512)S(1)} %get-tuple-element.5), channel_id=1, replica_groups=mesh['grp'=2,'ra'=4,'cb'=4] {'ra'}, use_global_device_ids=true, to_apply=%region_6.7 | all-reduce | flops 512 | bytes 4096 | tf_op jit(solution)/shard_map/psum | solution.py:239
  237.3 0.9 copy.28.scale_ref
  238.2 1.2 fusion.10.x_ref
  239.4 119.3 %hidden_1.1 = bf16[512,1024]{1,0:T(8,128)(2,1)} custom-call(bf16[512,1024]{1,0:T(8,128)(2,1)} %fusion.10.x_ref, f32[512,1]{1,0:T(8,128)} %copy.28.scale_ref, f32[8,2816]{1,0:T(8,128)} %get-tuple-element.13.coef_ref, bf16[1024,128]{1,0:T(8,128)(2,1)} %get-tuple-element.11.tg_ref, bf16[1024,128]{1,0:T(8,128)(2,1)} %get-tuple-element.20.tu_ref, ...), custom_call_target="tpu_custom_call" | custom-call | tf_op jit(solution)/shard_map/hidden_1/pallas_call | solution.py:183
  358.7 0.0 all-reduce.8.cloned.1.call-update
  358.7 34.4 %all-reduce.8.cloned.1.call-done = bf16[512,1024]{1,0:T(8,128)(2,1)} async-done(((bf16[512,1024]{1,0:T(8,128)(2,1)}), bf16[512,1024]{1,0:T(8,128)(2,1)}) %all-reduce.8.cloned.1.call-update) | async-done | bytes 1048592 | tf_op jit(solution)/shard_map/psum | solution.py:246
  393.2 1.5 fusion.4
  394.7 11.7 %psum.47 = f32[512]{0:T(512)S(1)} all-reduce(f32[512]{0:T(512)S(1)} %fusion.4), channel_id=1, replica_groups=mesh['grp'=2,'ra'=4,'cb'=4] {'ra'}, use_global_device_ids=true, to_apply=%region_9.10 | all-reduce | flops 512 | bytes 4096 | tf_op jit(solution)/shard_map/psum | solution.py:247
  406.4 2.7 fusion.7
  (10 shorter events, 0.1 us)
Async XLA Ops:
  6.5 207.2 %all-reduce.6.cloned.1.call-start = ((), (), s32[]{:S(2)}) async-start(), calls=%async_computation | async-start | bytes 2097152 | tf_op jit(solution)/shard_map/psum | solution.py:246
  43.4 16.4 %slice-start = ((bf16[2,1024,2752]{2,1,0:T(8,128)(2,1)}), bf16[2,1024,64]{2,1,0:T(8,128)(2,1)S(1)}, s32[]{:S(2)}) async-start(bf16[2,1024,2752]{2,1,0:T(8,128)(2,1)} %copy.23.wg_hbm), calls=%async_computation.2 | async-start | bytes 1048576 | tf_op jit(solution)/shard_map/slice | solution.py:227
  61.0 117.5 %copy-start.1 = (bf16[2,1024]{1,0:T(2,128)(2,1)S(1)}, bf16[2,1024]{1,0:T(2,128)(2,1)}, u32[]{:S(2)}) copy-start(bf16[2,1024]{1,0:T(2,128)(2,1)} %param.12) | copy-start | bytes 12292
  178.3 48.6 %copy-start = (bf16[512,1024]{1,0:T(8,128)(2,1)S(1)}, bf16[512,1024]{1,0:T(8,128)(2,1)}, u32[]{:S(2)}) copy-start(bf16[512,1024]{1,0:T(8,128)(2,1)} %param.10) | copy-start | bytes 3145732
  178.4 214.8 %all-reduce.8.cloned.1.call-start = ((), (), s32[]{:S(2)}) async-start(), calls=%async_computation.1 | async-start | bytes 2097152 | tf_op jit(solution)/shard_map/psum | solution.py:246
Sparse Core Ops, SparseCore 0:
  178.5 35.2 all-reduce.5
  358.9 34.2 all-reduce.7

commit v2 on v1

v2 whole, which is shorter than its diff:
```python
import functools

import jax
import jax.numpy as jnp
from jax import lax
from jax.experimental import pallas as pl
from jax.experimental.pallas import tpu as pltpu
from jax.sharding import PartitionSpec as P

LEN = 256
LANES = 128
SKEW = 2

epsilon = 1e-06
residual_scale = 0.5
MESH = pl.DeviceIdType.MESH


def hidden_kernel(
    layer, n, nx, nch, nfull, fl,
    state_ref, pre_ref, post_ref, coef_ref, wg_hbm, wu_hbm, wd_hbm,
    out_ref,
    w, wd, part, hid, acc, normed, scale, branch, pair_out, pair_in, xbuf, fresh, pre_sq, post_sq,
    wsem, wtail, wdsem, part_send, part_recv, hid_send, hid_recv,
    pre_send, pre_recv, post_send, post_recv, x_send, x_recv, pair_send, pair_recv,
):
    z = lax.axis_index("ra")
    k = lax.axis_index("cb")
    core, xi = k % 2, k // 2
    peer = k + 1 - 2 * core
    tokens, dl = state_ref.shape
    half = tokens // 2
    width = dl * n
    tail = fl - nfull * LANES

    def w_copies(j):
        cols = pl.ds(pl.multiple_of(j * LANES, LANES), LANES)
        return (
            pltpu.make_async_copy(
                wg_hbm.at[layer, cols], w.at[j, pl.ds(0, LANES)], wsem.at[0, j]),
            pltpu.make_async_copy(
                wu_hbm.at[layer, cols], w.at[j, pl.ds(LANES, LANES)], wsem.at[1, j]),
        )

    def tail_copies():
        cols = pl.ds(nfull * LANES, tail)
        return (
            pltpu.make_async_copy(
                wg_hbm.at[layer, cols], w.at[nfull, pl.ds(0, tail)], wtail.at[0]),
            pltpu.make_async_copy(
                wu_hbm.at[layer, cols], w.at[nfull, pl.ds(LANES, tail)], wtail.at[1]),
        )

    barrier = pltpu.get_barrier_semaphore()

    @pl.loop(1, n)
    def _(o):
        pl.semaphore_signal(
            barrier, inc=1, device_id={"ra": (z + o) % n}, device_id_type=MESH)

    pl.semaphore_signal(barrier, inc=1, device_id={"cb": peer}, device_id_type=MESH)
    for o in range(1, nx):
        pl.semaphore_signal(
            barrier, inc=1, device_id={"cb": (xi + o) % nx * 2 + core}, device_id_type=MESH)

    @pl.loop(0, nfull)
    def _(j):
        for copy in w_copies(j):
            copy.start()

    if tail:
        for copy in tail_copies():
            copy.start()
    wd_copy = pltpu.make_async_copy(wd_hbm.at[layer], wd.at[pl.ds(0, fl)], wdsem)
    wd_copy.start()

    eye = lax.broadcasted_iota(jnp.int32, (LANES, LANES), 0) == lax.broadcasted_iota(
        jnp.int32, (LANES, LANES), 1)

    def to_row(column):
        return jnp.sum(jnp.where(eye, column, 0.0), axis=0, keepdims=True)

    def to_column(row):
        return jnp.sum(jnp.where(eye, row, 0.0), axis=1, keepdims=True)

    def sq_copy(buf, send, recv, o, slot):
        return pltpu.make_async_remote_copy(
            src_ref=buf.at[slot], dst_ref=buf.at[slot],
            send_sem=send.at[o], recv_sem=recv.at[slot],
            device_id={"ra": (z + o) % n}, device_id_type=MESH)

    def sq_start(buf, send, recv):
        @pl.loop(1, n)
        def _(o):
            sq_copy(buf, send, recv, o, z).start()

    def sq_wait(buf, send, recv):
        @pl.loop(1, n)
        def _(o):
            sq_copy(buf, send, recv, o, (z + o) % n).wait_recv()

    def scale_of(buf, group):
        total = buf[0, group : group + 1, :]
        for slot in range(1, n):
            total = total + buf[slot, group : group + 1, :]
        return to_column(lax.rsqrt(total / width + epsilon))

    pre_sq[z] = jnp.zeros(pre_sq.shape[1:], jnp.float32)
    post_sq[z] = jnp.zeros(post_sq.shape[1:], jnp.float32)
    for group in range(tokens // LANES):
        rows = slice(group * LANES, (group + 1) * LANES)
        wide = state_ref[rows, :].astype(jnp.float32)
        pre_sq[z, group : group + 1, :] = to_row(jnp.sum(wide * wide, axis=1, keepdims=True))
        normed[rows, :] = (wide * pre_ref[...]).astype(normed.dtype)

    if tail:
        for lo in (0, LANES):
            w[nfull, lo + tail : lo + LANES, :] = jnp.zeros((LANES - tail, dl), w.dtype)
        wd[fl:, :] = jnp.zeros((nch * LANES - fl, wd.shape[1]), wd.dtype)
    acc[...] = jnp.zeros_like(acc)

    pl.semaphore_wait(barrier, n - 1 + nx)
    sq_start(pre_sq, pre_send, pre_recv)

    def place(d):
        if d == 0:
            return n - 1 - z, z - 1, z + 1
        return z, z + 1, z - 1

    def part_copy(d, j, target):
        return pltpu.make_async_remote_copy(
            src_ref=part.at[d, j], dst_ref=part.at[d, j],
            send_sem=part_send.at[d, j], recv_sem=part_recv.at[d, j],
            device_id={"ra": target}, device_id_type=MESH)

    def hid_copy(d, j, target):
        return pltpu.make_async_remote_copy(
            src_ref=hid.at[d, j], dst_ref=hid.at[d, j],
            send_sem=hid_send.at[d, j], recv_sem=hid_recv.at[d, j],
            device_id={"ra": target}, device_id_type=MESH)

    def conv(values, taps, bias):
        rows = lax.broadcasted_iota(jnp.int32, values.shape, 0) % LEN
        count = len(taps)
        result = taps[count - 1] * values
        for offset in range(1, count):
            moved = jnp.where(rows >= offset, pltpu.roll(values, offset, 0), 0.0)
            result = result + taps[count - 1 - offset] * moved
        return result + bias

    def add_down(d, j):
        rows = slice(d * half, (d + 1) * half)
        wrows = pl.ds(pl.multiple_of(j * LANES, LANES), LANES)
        acc[rows, :] += jnp.dot(hid[d, j], wd[wrows, :], preferred_element_type=jnp.float32)

    @pl.loop(0, nch + 2 * (n - 1) * SKEW)
    def _(s):
        @pl.when(s < nfull)
        def _():
            for copy in w_copies(s):
                copy.wait()

        @pl.when(s == 1)
        def _():
            wd_copy.wait()
            if tail:
                for copy in tail_copies():
                    copy.wait()

        @pl.when(s == (n - 1) * SKEW)
        def _():
            sq_wait(pre_sq, pre_send, pre_recv)
            for group in range(tokens // LANES):
                scale[group * LANES : (group + 1) * LANES, :] = scale_of(pre_sq, group)

        for d in range(2):
            p, nxt, prv = place(d)
            rows = slice(d * half, (d + 1) * half)
            c = s - p * SKEW

            @pl.when((c >= 0) & (c < nch))
            def _():
                own = lax.dot_general(
                    normed[rows, :], w[c], (((1,), (1,)), ((), ())),
                    preferred_element_type=jnp.float32)

                @pl.when(p == 0)
                def _():
                    part[d, c] = own.astype(part.dtype)
                    part_copy(d, c, nxt).start()

                @pl.when((p > 0) & (p < n - 1))
                def _():
                    part_copy(d, c, nxt).wait_recv()
                    part[d, c] = (part[d, c].astype(jnp.float32) + own).astype(part.dtype)
                    part_copy(d, c, nxt).start()

                @pl.when(p == n - 1)
                def _():
                    part_copy(d, c, prv).wait_recv()
                    total = (part[d, c].astype(jnp.float32) + own) * scale[rows, :]
                    coef = coef_ref[:, pl.ds(pl.multiple_of(c * LANES, LANES), LANES)]
                    m = coef.shape[0] // 2
                    row = [coef[i : i + 1, :] for i in range(2 * m)]
                    gate = conv(total[:, :LANES], row[: m - 1], row[m - 1])
                    up = conv(total[:, LANES:], row[m : 2 * m - 1], row[2 * m - 1])
                    hid[d, c] = (jax.nn.gelu(gate, approximate=True) * up).astype(hid.dtype)
                    hid_copy(d, c, prv).start()
                    add_down(d, c)

            e = s - (2 * (n - 1) - p) * SKEW

            @pl.when((p < n - 1) & (e >= 0) & (e < nch))
            def _():
                hid_copy(d, e, nxt).wait_recv()

                @pl.when(p > 0)
                def _():
                    hid_copy(d, e, prv).start()

                add_down(d, e)

    kept = pl.ds(pl.multiple_of(core * half, half), half)
    given = pl.ds(pl.multiple_of((1 - core) * half, half), half)
    pair_copy = pltpu.make_async_remote_copy(
        src_ref=pair_out, dst_ref=pair_in,
        send_sem=pair_send.at[0], recv_sem=pair_recv.at[0],
        device_id={"cb": peer}, device_id_type=MESH)
    pair_out[...] = acc[given, :].astype(pair_out.dtype)
    pair_copy.start()
    pair_copy.wait_recv()
    xbuf[xi] = (acc[kept, :] + pair_in[...].astype(jnp.float32)).astype(xbuf.dtype)

    def x_copy(o, slot):
        return pltpu.make_async_remote_copy(
            src_ref=xbuf.at[slot], dst_ref=xbuf.at[slot],
            send_sem=x_send.at[o], recv_sem=x_recv.at[slot],
            device_id={"cb": (xi + o) % nx * 2 + core}, device_id_type=MESH)

    for o in range(1, nx):
        x_copy(o, xi).start()
    for o in range(1, nx):
        x_copy(o, (xi + o) % nx).wait_recv()
    for group in range(half // LANES):
        rows = slice(group * LANES, (group + 1) * LANES)
        total = xbuf[0, rows, :].astype(jnp.float32)
        for i in range(1, nx):
            total = total + xbuf[i, rows, :].astype(jnp.float32)
        branch[rows, :] = total
        post_sq[z, group : group + 1, :] = to_row(jnp.sum(total * total, axis=1, keepdims=True))
    sq_start(post_sq, post_send, post_recv)
    sq_wait(post_sq, post_send, post_recv)
    for group in range(half // LANES):
        rows = slice(group * LANES, (group + 1) * LANES)
        own = pl.ds(pl.multiple_of(core * half + group * LANES, LANES), LANES)
        fresh[own, :] = (
            residual_scale * state_ref[own, :].astype(jnp.float32)
            + branch[rows, :] * scale_of(post_sq, group) * post_ref[...]
        ).astype(fresh.dtype)

    state_copy = pltpu.make_async_remote_copy(
        src_ref=fresh.at[kept], dst_ref=fresh.at[kept],
        send_sem=pair_send.at[1], recv_sem=pair_recv.at[1],
        device_id={"cb": peer}, device_id_type=MESH)
    state_copy.start()
    out_ref[kept, :] = fresh[kept, :]
    pltpu.make_async_remote_copy(
        src_ref=fresh.at[given], dst_ref=fresh.at[given],
        send_sem=pair_send.at[1], recv_sem=pair_recv.at[1],
        device_id={"cb": peer}, device_id_type=MESH).wait_recv()
    out_ref[given, :] = fresh[given, :]

    pair_copy.wait_send()
    state_copy.wait_send()
    for o in range(1, nx):
        x_copy(o, xi).wait_send()

    @pl.loop(1, n)
    def _(o):
        sq_copy(pre_sq, pre_send, pre_recv, o, z).wait_send()
        sq_copy(post_sq, post_send, post_recv, o, z).wait_send()

    for d in range(2):
        p, nxt, prv = place(d)

        @pl.loop(0, nch)
        def _(j):
            @pl.when(p < n - 1)
            def _():
                part_copy(d, j, nxt).wait_send()

            @pl.when(p > 0)
            def _():
                hid_copy(d, j, prv).wait_send()


def sublayer(layer, n, nx, state, pre, post, coef, gate_weight, up_weight, down_weight):
    tokens, dl = state.shape
    fl = gate_weight.shape[1]
    nfull = fl // LANES
    nch = -(-fl // LANES)
    half = tokens // 2
    sq_rows = -(-(tokens // LANES) // 8) * 8
    vmem = pl.BlockSpec(memory_space=pltpu.VMEM)
    hbm = pl.BlockSpec(memory_space=pl.ANY)
    dma = pltpu.SemaphoreType.DMA
    bf16, f32 = jnp.bfloat16, jnp.float32
    return pl.pallas_call(
        functools.partial(hidden_kernel, layer, n, nx, nch, nfull, fl),
        out_shape=jax.ShapeDtypeStruct((tokens, dl), bf16),
        in_specs=[vmem] * 4 + [hbm] * 3,
        out_specs=vmem,
        scratch_shapes=[
            pltpu.VMEM((nch, 2 * LANES, dl), bf16),
            pltpu.VMEM((nch * LANES, dl), bf16),
            pltpu.VMEM((2, nch, half, 2 * LANES), bf16),
            pltpu.VMEM((2, nch, half, LANES), bf16),
            pltpu.VMEM((tokens, dl), f32),
            pltpu.VMEM((tokens, dl), bf16),
            pltpu.VMEM((tokens, 1), f32),
            pltpu.VMEM((half, dl), f32),
            pltpu.VMEM((half, dl), bf16),
            pltpu.VMEM((half, dl), bf16),
            pltpu.VMEM((nx, half, dl), bf16),
            pltpu.VMEM((tokens, dl), bf16),
            pltpu.VMEM((n, sq_rows, LANES), f32),
            pltpu.VMEM((n, sq_rows, LANES), f32),
            dma((2, nch)),
            dma((2,)),
            dma,
            dma((2, nch)),
            dma((2, nch)),
            dma((2, nch)),
            dma((2, nch)),
            dma((n,)),
            dma((n,)),
            dma((n,)),
            dma((n,)),
            dma((nx,)),
            dma((nx,)),
            dma((2,)),
            dma((2,)),
        ],
        compiler_params=pltpu.CompilerParams(
            collective_id=layer, has_side_effects=True, vmem_limit_bytes=56 * 1024 * 1024
        ),
        name=f"hidden_{layer}",
    )(state, pre, post, coef, gate_weight, up_weight, down_weight)


def local(
    n,
    nx,
    tokens,
    pre_gain,
    post_gain,
    gate_weight,
    up_weight,
    gate_taps,
    up_taps,
    gate_bias,
    up_bias,
    down_weight,
):
    padding = -gate_weight.shape[2] % LANES
    coefs = jnp.concatenate(
        [gate_taps, gate_bias[:, None], up_taps, up_bias[:, None]], axis=1
    ).astype(jnp.float32)
    coefs = jnp.pad(coefs, ((0, 0), (0, 0), (0, padding)))
    pre, post = pre_gain.astype(jnp.float32), post_gain.astype(jnp.float32)
    gate_cols = jnp.swapaxes(gate_weight, 1, 2)
    up_cols = jnp.swapaxes(up_weight, 1, 2)
    state = tokens
    for layer in range(gate_weight.shape[0]):
        state = sublayer(
            layer, n, nx, state, pre[layer : layer + 1], post[layer : layer + 1], coefs[layer],
            gate_cols, up_cols, down_weight,
        )
    return state


def solution(mesh):
    in_specs = (
        P("grp", "ra"),
        P(None, "ra"),
        P(None, "ra"),
        P(None, "ra", "cb"),
        P(None, "ra", "cb"),
        P(None, None, "cb"),
        P(None, None, "cb"),
        P(None, "cb"),
        P(None, "cb"),
        P(None, "cb", "ra"),
    )
    body = functools.partial(local, mesh.shape["ra"], mesh.shape["cb"] // 2)
    return jax.shard_map(
        body, mesh=mesh, in_specs=in_specs, out_specs=P("grp", "ra"), check_vma=False
    )
```

time: 417 us -> 284 us (0.68)
  waiting for transfers between devices: 69.8 us -> 0 us
  blocking collectives: 45.2 us -> 0 us
  Pallas kernels: 237 us -> 276 us
  local copies, waits for them, and re-layouts: 38.4 us -> 7.33 us
  between operations: 13.5 us -> 0.04 us
  other arithmetic: 12.3 us -> 0.11 us
    psum x2 -> x0, waiting for transfers between devices: 69.7 us -> none  [local(): branch = lax.psum(partial_value, 'cb').astype(jnp.float32)]
    psum x4 -> x0, blocking collectives: 45.2 us -> none  [the longest x2 23.4 us: local(): post_total = lax.psum(jnp.sum(branch * branch, axis=1), 'ra')]
    pallas_call x2, Pallas kernels: 237 us -> 276 us  [sublayer(): pl.pallas_call(functools.partial(hidden_kernel, layer, n, nx, nch, nfull,...]
    unnamed x8 -> x3, local copies, waits for them, and re-layouts: 32.3 us -> 3.83 us
    reduce_sum x4 -> x0, other arithmetic: 7.45 us -> none  [the longest x2 4.45 us: local(): pre_total = lax.psum(jnp.sum(widened * widened, axis=1), 'ra')]
  transfers between devices with their start and end apart: 2 -> 0, of which waited for: 2 -> 0; matrix products, arithmetic and copies ran while one was open for 0% -> 0% of each run, Pallas kernels for 0% -> 0%
where the time goes in v2:
time: 284 us
  Pallas kernels  276 us (97%)
  local copies, waits for them, and re-layouts  7.33 us (3%)
    pallas_call x2, Pallas kernels, sublayer(): pl.pallas_call(functools.partial(hidden_kernel, layer, n, nx, nch, nfull,...  276 us

profile of v2, /device:TPU:0, one launch (start us, length us, event | category | flops | bytes accessed | tf_op | source)
XLA Modules:
  0.0 283.8 jit_solution(1047870244427706999)
XLA Ops:
  0.0 1.4 fusion.8
  1.4 0.7 copy.14
  2.1 0.7 copy.16
  2.8 0.8 copy.13
  3.6 0.8 copy.15
  4.4 0.1 fusion.7
  4.5 0.7 slice_bitcast_fusion
  5.2 138.9 %hidden_0.1.state_ref = bf16[512,1024]{1,0:T(8,128)(2,1)} custom-call(bf16[512,1024]{1,0:T(8,128)(2,1)} %state_ref.1, f32[1,1024]{1,0:T(1,128)} %get-tuple-element.11.pre_ref, f32[1,1024]{1,0:T(1,128)} %get-tuple-element.8.post_ref, f32[8,2816]{1,0:T(8,128)} %get-tuple-element.6.coef_ref, bf16[2,2752,1024]{2,1,0:T(8,128)(2,1)} %bitcast.8, ...), custom_call_target="tpu_custom_call" | custom-call | tf_op jit(solution)/shard_map/hidden_0/pallas_call | solution.py:308
  144.1 137.5 %hidden_1.1 = bf16[512,1024]{1,0:T(8,128)(2,1)} custom-call(bf16[512,1024]{1,0:T(8,128)(2,1)} %hidden_0.1.state_ref, f32[1,1024]{1,0:T(1,128)} %get-tuple-element.12.pre_ref, f32[1,1024]{1,0:T(1,128)} %get-tuple-element.7.post_ref, f32[8,2816]{1,0:T(8,128)} %get-tuple-element.5.coef_ref, bf16[2,2752,1024]{2,1,0:T(8,128)(2,1)} %bitcast.9, ...), custom_call_target="tpu_custom_call" | custom-call | tf_op jit(solution)/shard_map/hidden_1/pallas_call | solution.py:308
  281.6 2.3 copy.18
